TPU v7x, 32 devices: a whole 2x2x4 slice. The times are simulated.
32 devices in a mesh: sp: 8 (over z, y), tp: 4 (over x, core).
Axes of the slice: x: 2, y: 2, z: 4, core: 2. Of those that a mesh axis runs over, the one named last changes fastest.
Arguments:
- memory_queries: bfloat16 [2048, 768], P('sp', 'tp'), may hold values from -6 to 6
- memory_keys: bfloat16 [2048, 768], P('sp', 'tp'), may hold values from -6 to 6
- memory_values: bfloat16 [2048, 768], P('sp', 'tp'), may hold values from -6 to 6
- output_gate_preactivation: bfloat16 [2048, 768], P('sp', 'tp'), may hold values from -6 to 6
- log_input_gate: float32 [8, 2048], P('tp', 'sp'), may hold values from -4 to 300
- forget_preactivation: float32 [8, 2048], P('tp', 'sp'), may hold values from -5 to 5
- head_forget_bias: float32 [8], P('tp'), may hold values from 3 to 16
- forget_extra_boost: float32 [8, 2048], P('tp', 'sp'), may hold values from -2 to 0
- head_norm_gain: float32 [768], P('tp'), may hold values from 0.1 to 1.9
- memory_output_weight: bfloat16 [768, 2048], replicated, may hold values from -0.21875 to 0.21875
- residual: bfloat16 [2048, 2048], P('sp'), may hold values from -6 to 6
- expert_norm_gain: float32 [2048], replicated, may hold values from 0.1 to 1.9
- routes: int32 [2048, 4], P('sp'), may hold values from 0 to 31, all different within a row; in each aligned block of 256 rows (0 to 255, 256 to 511, ...) at most 64 rows name the same one
- router_weight_matrix: float32 [2048, 4], P('sp'), may hold values from 0.1 to 1
- routed_gate_weight: bfloat16 [32, 2048, 512], P('sp', None, 'tp'), may hold values from -0.125 to 0.125
- routed_up_weight: bfloat16 [32, 2048, 512], P('sp', None, 'tp'), may hold values from -0.125 to 0.125
- routed_down_weight: bfloat16 [32, 512, 2048], P('sp', 'tp'), may hold values from -0.25 to 0.25
- shared_gate_weight: bfloat16 [2048, 512], P(None, 'tp'), may hold values from -0.125 to 0.125
- shared_up_weight: bfloat16 [2048, 512], P(None, 'tp'), may hold values from -0.125 to 0.125
- shared_down_weight: bfloat16 [512, 2048], P('tp'), may hold values from -0.25 to 0.25
Outputs:
- updated: bfloat16 [2048, 2048], P('sp', 'tp')
Inputs may be any that keep to these rules, and one draw needn't show every extreme that they name: `routes`: each row names 4 different experts. In each aligned block of 256 rows (the rows of one index of sp) no expert is named by more than 64 rows, a bound that some block reaches.
All inputs are finite; a program needn't handle non-finite values.
Results may differ from a plain program's by a relative error of at most 0.0085.
Values may be sent and summed in bfloat16 or wider, within the bound.
A program may use at most 128 MiB of HBM per device.

v0:
```python
import jax
import jax.numpy as jnp
from jax import lax
from jax.sharding import PartitionSpec as P

NEG_LARGE = -1e30
EPSILON = 1e-06


def entering(shard, axis, combine, identity):
    count, here = (lax.axis_size(axis), lax.axis_index(axis))
    everything = jax.tree.map(lambda part: lax.all_gather(part, axis), shard)
    start = jax.tree.map(
        lambda part, zero: jnp.broadcast_to(jnp.asarray(zero, part.dtype), part.shape),
        shard,
        identity,
    )

    def step(k, before):
        reached = k < here
        new = combine(before, jax.tree.map(lambda part: part[k], everything))
        return jax.tree.map(lambda a, b: jnp.where(reached, a, b), new, before)

    return lax.fori_loop(0, count, step, start)


def join_states(earlier, later):
    memory_a, top_a, total_a = earlier
    memory_b, top_b, total_b = later
    joined = jnp.maximum(total_b + top_a, top_b)
    carry_weight = jnp.exp(total_b + top_a - joined)
    own_weight = jnp.exp(top_b - joined)
    memory = carry_weight[:, None, None] * memory_a + own_weight[:, None, None] * memory_b
    return (memory, joined, total_a + total_b)


def body(
    memory_queries,
    memory_keys,
    memory_values,
    output_gate_preactivation,
    log_input_gate,
    forget_preactivation,
    head_forget_bias,
    forget_extra_boost,
    head_norm_gain,
    memory_output_weight,
    residual,
    expert_norm_gain,
    routes,
    router_weight_matrix,
    routed_gate_weight,
    routed_up_weight,
    routed_down_weight,
    shared_gate_weight,
    shared_up_weight,
    shared_down_weight,
):
    tokens_here = memory_queries.shape[0]
    heads_here = log_input_gate.shape[0]
    head_size = memory_queries.shape[1] // heads_here
    scale = head_size ** (-0.5)
    queries = memory_queries.reshape(tokens_here, heads_here, head_size)
    keyset = memory_keys.reshape(tokens_here, heads_here, head_size)
    valueset = memory_values.reshape(tokens_here, heads_here, head_size)
    forget_log_gate = (
        jax.nn.log_sigmoid(forget_preactivation + head_forget_bias[:, None]) + forget_extra_boost
    )
    cumul = jnp.cumsum(forget_log_gate, axis=1)
    causal = jnp.tril(jnp.ones((tokens_here, tokens_here), bool))
    d_log = jnp.where(
        causal[None], cumul[:, :, None] - cumul[:, None, :] + log_input_gate[:, None, :], NEG_LARGE
    )
    ending = cumul[:, -1]
    w_log = ending[:, None] - cumul + log_input_gate
    local_top = jnp.max(w_log, axis=1)
    w_end = jnp.exp(w_log - local_top[:, None])
    keys_float = keyset.astype(jnp.float32)
    values_float = valueset.astype(jnp.float32)
    local_memory = jnp.einsum(
        "hs,shd,she->hde", w_end, keys_float, values_float, precision=lax.Precision.HIGHEST
    )
    identity = (
        jnp.zeros_like(local_memory),
        jnp.full_like(local_top, NEG_LARGE),
        jnp.zeros_like(ending),
    )
    memory, stabil, _ = entering((local_memory, local_top, ending), "sp", join_states, identity)
    g_log = cumul + stabil[:, None]
    top = jnp.maximum(g_log, jnp.max(d_log, axis=2))
    scores = jnp.einsum("thd,shd->hts", queries, keyset, preferred_element_type=jnp.float32) * scale
    weights = scores * jnp.exp(d_log - top[:, :, None])
    inter = jnp.exp(g_log - top)
    q_scaled = queries.astype(jnp.float32) * scale
    numer = jnp.einsum(
        "hts,shd->thd", weights.astype(jnp.bfloat16), valueset, preferred_element_type=jnp.float32
    )
    hidden = numer + inter.T[:, :, None] * jnp.einsum(
        "thd,hde->the", q_scaled, memory, precision=lax.Precision.HIGHEST
    )
    hidden = hidden * lax.rsqrt(jnp.mean(hidden * hidden, axis=2, keepdims=True) + EPSILON)
    token_mixing = (
        hidden.reshape(tokens_here, heads_here * head_size)
        * head_norm_gain
        * jax.nn.sigmoid(output_gate_preactivation.astype(jnp.float32))
    ).astype(jnp.bfloat16)
    model_width = residual.shape[1]
    mixed = jnp.dot(
        lax.all_gather(token_mixing, "tp", axis=1, tiled=True),
        memory_output_weight,
        preferred_element_type=jnp.float32,
    )
    stream = residual.astype(jnp.float32) + mixed
    normed = (
        stream
        * lax.rsqrt(jnp.mean(stream * stream, axis=1, keepdims=True) + EPSILON)
        * expert_norm_gain
    ).astype(jnp.bfloat16)
    sp_count = lax.axis_size("sp")
    tp_count = lax.axis_size("tp")
    tp_index = lax.axis_index("tp")
    local_experts = routed_gate_weight.shape[0]
    experts_total = local_experts * sp_count
    top_count = routes.shape[1]
    capacity = 2 * tokens_here * top_count // experts_total
    width_share = model_width // tp_count
    flat_routes = routes.reshape(-1)
    onehot = (flat_routes[:, None] == jnp.arange(experts_total, dtype=jnp.int32)[None, :]).astype(
        jnp.int32
    )
    earlier_count = jnp.cumsum(onehot, axis=0) - onehot
    slot_index = jnp.sum(earlier_count * onehot, axis=1)
    position = flat_routes * capacity + slot_index
    owner = jnp.arange(flat_routes.shape[0], dtype=jnp.int32) // top_count
    slot_token = (
        jnp.full((experts_total * capacity,), tokens_here, jnp.int32).at[position].set(owner)
    )
    padded = jnp.concatenate([normed, jnp.zeros((1, model_width), jnp.bfloat16)], axis=0)
    shared_hidden = (
        jax.nn.silu(jnp.dot(normed, shared_gate_weight, preferred_element_type=jnp.float32))
        * jnp.dot(normed, shared_up_weight, preferred_element_type=jnp.float32)
    ).astype(jnp.bfloat16)
    shared_partial = jnp.dot(shared_hidden, shared_down_weight, preferred_element_type=jnp.float32)
    stream_share = lax.dynamic_slice_in_dim(stream, tp_index * width_share, width_share, 1)
    group_count = local_experts // tp_count
    whole_gate, whole_up = (
        lax.all_to_all(routed_gate_weight, "tp", split_axis=0, concat_axis=2, tiled=True),
        lax.all_to_all(routed_up_weight, "tp", split_axis=0, concat_axis=2, tiled=True),
    )
    whole_down = lax.all_to_all(routed_down_weight, "tp", split_axis=0, concat_axis=1, tiled=True)
    slot_table = slot_token.reshape(sp_count, local_experts, capacity)
    chosen = lax.dynamic_slice_in_dim(slot_table, tp_index * group_count, group_count, 1)
    outgoing = jnp.take(padded, chosen.reshape(-1), axis=0).reshape(
        sp_count, group_count, capacity, model_width
    )
    arrived = lax.all_to_all(outgoing, "sp", split_axis=0, concat_axis=0, tiled=True)
    gate_vals = jnp.einsum(
        "secd,edf->secf", arrived, whole_gate, preferred_element_type=jnp.float32
    )
    up_vals = jnp.einsum("secd,edf->secf", arrived, whole_up, preferred_element_type=jnp.float32)
    expert_hidden = (jax.nn.silu(gate_vals) * up_vals).astype(jnp.bfloat16)
    hidden_width = whole_down.shape[1]
    group_width = hidden_width // tp_count
    expert_sum = jnp.zeros(arrived.shape[:3] + (model_width,), jnp.float32)
    for index in range(tp_count):
        piece = jnp.einsum(
            "secf,efd->secd",
            expert_hidden[..., index * group_width : (index + 1) * group_width],
            whole_down[:, index * group_width : (index + 1) * group_width, :],
            preferred_element_type=jnp.float32,
        )
        expert_sum = expert_sum + piece.astype(jnp.bfloat16).astype(jnp.float32)
    expert_rows = expert_sum.astype(jnp.bfloat16)
    back = lax.all_to_all(expert_rows, "sp", split_axis=0, concat_axis=0, tiled=True)
    back_flat = back.reshape(sp_count * group_count * capacity, model_width)
    owner_sp = flat_routes // local_experts
    local_slot = flat_routes % local_experts - tp_index * group_count
    belongs = (local_slot >= 0) & (local_slot < group_count)
    local_position = jnp.where(
        belongs, (owner_sp * group_count + local_slot) * capacity + slot_index, 0
    )
    picked = jnp.take(back_flat, local_position, axis=0).reshape(
        tokens_here, top_count, model_width
    )
    kept_weight = jnp.where(belongs.reshape(tokens_here, top_count), router_weight_matrix, 0.0)
    routed_partial = jnp.sum(kept_weight[:, :, None] * picked.astype(jnp.float32), axis=1)
    shared_rounded = shared_partial.astype(jnp.bfloat16).astype(jnp.float32)
    combined = lax.psum_scatter(
        (routed_partial + shared_rounded).astype(jnp.bfloat16),
        "tp",
        scatter_dimension=1,
        tiled=True,
    ).astype(jnp.float32)
    return (stream_share + combined).astype(jnp.bfloat16)


def solution(mesh):
    in_specs = (
        P("sp", "tp"),
        P("sp", "tp"),
        P("sp", "tp"),
        P("sp", "tp"),
        P("tp", "sp"),
        P("tp", "sp"),
        P("tp"),
        P("tp", "sp"),
        P("tp"),
        P(),
        P("sp", None),
        P(),
        P("sp", None),
        P("sp", None),
        P("sp", None, "tp"),
        P("sp", None, "tp"),
        P("sp", "tp", None),
        P(None, "tp"),
        P(None, "tp"),
        P("tp", None),
    )
    out_specs = P("sp", "tp")
    return jax.shard_map(body, mesh=mesh, in_specs=in_specs, out_specs=out_specs, check_vma=False)
```

profile of v0, /device:TPU:0, one launch (start us, length us, event | category | flops | bytes accessed | tf_op | source)
XLA Modules:
  0.0 371.8 jit_solution(7712659421824547058)
XLA Ops:
  6.5 4.7 %all-to-all-start.1 = ((bf16[4,2048,128]{2,1,0:T(8,128)(2,1)}), bf16[4,2048,128]{2,1,0:T(8,128)(2,1)}, u32[]{:S(2)}, u32[]{:S(2)}) async-start(bf16[4,2048,128]{2,1,0:T(8,128)(2,1)} %param.36), calls=%async_computation.1 | async-start | bytes 4194304 | tf_op jit(solution)/shard_map/all_to_all | solution.py:147
  12.3 0.8 fusion.75
  13.9 0.8 reduce-window.15
  15.6 0.9 fusion.82
  17.0 1.1 fusion.46
  18.2 35.5 %all-gather.2 = f32[16,96,96]{2,1,0:T(8,128)} all-gather(f32[2,96,96]{2,1,0:T(8,128)S(1)} %fusion.46), channel_id=4, replica_groups=mesh['sp'=8,'tp'=4] {'sp'}, dimensions={0}, use_global_device_ids=true | all-gather | bytes 663552 | tf_op jit(solution)/shard_map/all_gather | solution.py:12
  53.7 1.2 dynamic-slice
  55.5 0.8 dynamic-update-slice.1
  56.3 0.8 dynamic-update-slice
  57.2 21.7 %all-reduce.3 = (f32[16]{0:T(128)S(1)}, f32[16]{0:T(128)S(1)}) all-reduce(f32[16]{0:T(128)S(1)} %dynamic-update-slice, f32[16]{0:T(128)S(1)} %dynamic-update-slice.1), channel_id=2, replica_groups=mesh['sp'=8,'tp'=4] {'sp'}, use_global_device_ids=true, to_apply=%add.1 | all-reduce | flops 32 | bytes 256
  79.1 8.4 %while.16 = (s32[]{:T(128)}, f32[2,96,96]{2,1,0:T(8,128)S(1)}, f32[2]{0:T(128)S(1)}, s32[]{:T(128)}, f32[8,2]{1,0:T(8,128)S(1)}, /*index=5*/f32[8,2]{1,0:T(8,128)S(1)}, f32[8,2,96,96]{3,2,1,0:T(8,128)}, s32[]{:T(128)}, s32[]{:T(128)}) while((s32[]{:T(128)}, f32[2,96,96]{2,1,0:T(8,128)S(1)}, f32[2]{0:T(128)S(1)}, s32[]{:T(128)}, ...), condition=%wide.region_4.5_spmd.clone, body=%wide.region_3.4_spmd.clone.sunk | while | flops 92178 | bytes 221399 | solution.py:24
  79.2 1.0 fusion.99
  80.2 1.0 fusion.99
  81.3 1.0 fusion.99
  82.3 1.0 fusion.99
  83.4 1.0 fusion.99
  84.4 1.0 fusion.99
  85.5 1.0 fusion.99
  86.5 1.0 fusion.99
  87.5 1.5 fusion.34
  89.7 15.7 %reduce-window.16 = s32[32,8,128]{2,1,0:T(8,128)S(1)} reduce-window(s32[32,8,128]{2,1,0:T(8,128)} %fusion.63, s32[]{:T(128)} %constant.130.clone.1), window={size=1x1x128 pad=0_0x0_0x127_0}, to_apply=%region_7.8 | reduce-window | flops 4161536 | bytes 262148 | tf_op jit(solution)/shard_map/reduce-window.2
  106.2 1.0 copy.53
  107.3 0.8 broadcast_add_fusion
  108.1 0.8 exponential_bitcast_fusion
  108.9 2.2 fusion.30
  111.0 0.9 fusion.56
  112.0 2.0 multiply_reduce_fusion.2
  114.1 4.3 %scatter_custom_fusion = s32[2048]{0:T(1024)S(1)} fusion(s32[1024]{0:T(1024)S(1)} %bitcast.194, s32[1024]{0:T(1024)S(1)} %add_select_fusion.4, s32[]{:T(128)} %constant.147.clone.1), kind=kCustom, calls=%fused_computation.130 | custom fusion | bytes 8196 | tf_op jit(solution)/shard_map/scatter | solution.py:136
  119.7 0.9 broadcast_multiply_fusion
  120.7 0.8 fusion.43
  121.5 7.0 %all_gather.23 = bf16[256,768]{0,1:T(8,128)(2,1)S(1)} all-gather(bf16[256,192]{0,1:T(8,128)(2,1)S(1)} %fusion.43), channel_id=1, replica_groups=mesh['sp'=8,'tp'=4] {'tp'}, dimensions={1}, use_global_device_ids=true | all-gather | bytes 491520 | tf_op jit(solution)/shard_map/all_gather | solution.py:109
  128.4 3.6 multiply_reduce_fusion.1
  132.1 4.6 %all-to-all-start.2 = ((bf16[4,2048,128]{2,1,0:T(8,128)(2,1)}), bf16[4,2048,128]{2,1,0:T(8,128)(2,1)}, u32[]{:S(2)}, u32[]{:S(2)}) async-start(bf16[4,2048,128]{2,1,0:T(8,128)(2,1)} %param.37), calls=%async_computation.2 | async-start | bytes 4194304 | tf_op jit(solution)/shard_map/all_to_all | solution.py:148
  136.7 1.8 multiply_convert_fusion
  138.6 1.0 copy-done.1
  139.6 1.1 concatenate.3
  140.7 6.6 %gather_fusion = bf16[512,2048]{1,0:T(8,128)(2,1)} fusion(bf16[257,2048]{1,0:T(8,128)(2,1)} %concatenate.3, s32[1024]{0:T(1024)S(1)} %pad_clamp_fusion), kind=kCustom, calls=%fused_computation | custom fusion | bytes 4196352 | tf_op jit(solution)/shard_map/jit(_take)/gather | solution.py:153
  147.4 3.1 broadcast_select_fusion.2
  150.5 11.9 %all-to-all-done.2 = bf16[4,2048,128]{2,1,0:T(8,128)(2,1)} async-done(((bf16[4,2048,128]{2,1,0:T(8,128)(2,1)}), bf16[4,2048,128]{2,1,0:T(8,128)(2,1)}, u32[]{:S(2)}, u32[]{:S(2)}) %all-to-all-start.2) | async-done | bytes 2097184 | tf_op jit(solution)/shard_map/all_to_all | solution.py:148
  162.4 52.6 %all_to_all.52 = bf16[8,1,64,2048]{3,2,1,0:T(8,128)(2,1)} all-to-all(bf16[8,1,64,2048]{3,2,1,0:T(8,128)(2,1)} %broadcast_select_fusion.2), channel_id=1, replica_groups=mesh['sp'=8,'tp'=4] {'sp'}, dimensions={0} | all-to-all | bytes 4194304 | tf_op jit(solution)/shard_map/all_to_all | solution.py:156
  215.0 4.6 %all-to-all-start.3 = ((bf16[4,128,2048]{2,1,0:T(8,128)(2,1)}), bf16[4,128,2048]{2,1,0:T(8,128)(2,1)}, u32[]{:S(2)}, u32[]{:S(2)}) async-start(bf16[4,128,2048]{2,1,0:T(8,128)(2,1)} %param.38), calls=%async_computation.3 | async-start | bytes 4194304 | tf_op jit(solution)/shard_map/all_to_all | solution.py:150
  219.6 4.7 %copy.57 = bf16[1,2048,4,128]{3,2,1,0:T(4,128)(2,1)} copy(bf16[1,2048,4,128]{3,1,2,0:T(8,128)(2,1)} %bitcast.20) | data formatting | bytes 4194304 | tf_op jit(solution)/shard_map/all_to_all | solution.py:147
  224.3 4.1 %reshape.484 = bf16[2048,512,1]{1,0,2:T(8,128)(2,1)} reshape(bf16[1,2048,4,128]{3,2,1,0:T(4,128)(2,1)} %copy.57) | data formatting | bytes 4194304 | tf_op jit(solution)/shard_map/reshape.23
  228.4 4.6 %copy.58 = bf16[1,2048,4,128]{3,2,1,0:T(4,128)(2,1)} copy(bf16[1,2048,4,128]{3,1,2,0:T(8,128)(2,1)} %bitcast.27) | data formatting | bytes 4194304 | tf_op jit(solution)/shard_map/all_to_all | solution.py:148
  233.0 4.1 %reshape.485 = bf16[2048,512,1]{1,0,2:T(8,128)(2,1)} reshape(bf16[1,2048,4,128]{3,2,1,0:T(4,128)(2,1)} %copy.58) | data formatting | bytes 4194304 | tf_op jit(solution)/shard_map/reshape.26
  237.2 3.6 fusion.13
  240.8 2.1 fusion.22
  242.9 2.2 all-to-all-done.3
  245.2 1.9 convolution_convert_fusion.1
  247.0 1.7 convolution_convert_fusion.2
  248.8 1.7 convolution_convert_fusion
  250.5 3.5 fusion.5
  254.1 4.5 %all-to-all-start.4 = ((bf16[8,1,64,2048]{3,2,1,0:T(8,128)(2,1)}), bf16[8,1,64,2048]{3,2,1,0:T(8,128)(2,1)}, u32[]{:S(2)}, u32[]{:S(2)}) async-start(bf16[8,1,64,2048]{3,2,1,0:T(8,128)(2,1)} %fusion.5), calls=%async_computation.4 | async-start | bytes 4194304 | tf_op jit(solution)/shard_map/all_to_all | solution.py:174
  259.0 0.8 copy.47
  259.9 1.6 compare_and_fusion
  261.5 0.8 fusion.64
  262.3 1.8 fusion.83
  264.1 42.7 %all-to-all-done.4 = bf16[8,1,64,2048]{3,2,1,0:T(8,128)(2,1)} async-done(((bf16[8,1,64,2048]{3,2,1,0:T(8,128)(2,1)}), bf16[8,1,64,2048]{3,2,1,0:T(8,128)(2,1)}, u32[]{:S(2)}, u32[]{:S(2)}) %all-to-all-start.4) | async-done | bytes 2097184 | tf_op jit(solution)/shard_map/all_to_all | solution.py:174
  306.8 10.7 %gather_fusion.1 = bf16[1024,2048]{1,0:T(8,128)(2,1)} fusion(bf16[512,2048]{1,0:T(8,128)(2,1)} %bitcast.48, s32[1024]{0:T(1024)S(1)} %broadcast_clamp_fusion), kind=kCustom, calls=%fused_computation.1 | custom fusion | bytes 8392704 | tf_op jit(solution)/shard_map/jit(_take)/gather | solution.py:182
  317.5 7.2 %gather.15 = bf16[256,4,2048]{2,1,0:T(4,128)(2,1)} reshape(bf16[1024,2048]{1,0:T(8,128)(2,1)} %gather_fusion.1) | data formatting | bytes 8388608 | tf_op jit(solution)/shard_map/jit(_take)/gather | solution.py:182
  324.7 11.3 %multiply_reduce_fusion = f32[256,2048]{1,0:T(8,128)} fusion(bf16[256,4,2048]{2,1,0:T(4,128)(2,1)} %gather.15, f32[256,4]{1,0:T(8,128)S(1)} %fusion.64, pred[256,4]{1,0:T(8,128)(4,1)S(1)} %copy-done.6), kind=kLoop, calls=%fused_computation.15 | loop fusion | flops 7864320 | bytes 6296576 | tf_op jit(solution)/shard_map/reduce_sum | solution.py:186
  336.0 4.0 %fusion.8 = bf16[256,2048]{1,0:T(8,128)(2,1)} fusion(f32[256,2048]{1,0:T(8,128)} %multiply_reduce_fusion, bf16[128,2048]{1,0:T(8,128)(2,1)} %param.41, bf16[256,2048]{1,0:T(8,128)(2,1)} %copy-done.1, bf16[2048,128]{1,0:T(8,128)(2,1)} %param.40, f32[256,128]{1,0:T(8,128)S(1)} %fusion.83), kind=kOutput, calls=%fused_computation.26 | convolution fusion | flops 270729216 | bytes 5373952 | tf_op jit(solution)/shard_map/dot_general | solution.py:143
  340.0 23.0 %reduce-scatter.2.cloned.1.call-done = bf16[256,512]{1,0:T(8,128)(2,1)} async-done(((bf16[256,2048]{1,0:T(8,128)(2,1)}), bf16[256,512]{1,0:T(8,128)(2,1)}) %reduce-scatter.2.cloned.1.call-update) | async-done | bytes 262160 | tf_op jit(solution)/shard_map/reduce_scatter | solution.py:188
  363.0 1.9 add_convert_fusion.1
  (90 shorter events, 7.4 us)
Async XLA Ops:
  6.5 121.9 %copy-start = (bf16[768,2048]{1,0:T(8,128)(2,1)S(1)}, bf16[768,2048]{1,0:T(8,128)(2,1)}, u32[]{:S(2)}) copy-start(bf16[768,2048]{1,0:T(8,128)(2,1)} %param.31) | copy-start | bytes 9437188
  6.5 4.8 %copy-start.10 = (s32[256,4]{0,1:T(4,128)S(1)}, s32[256,4]{0,1:T(4,128)}, u32[]{:S(2)}) copy-start(s32[256,4]{0,1:T(4,128)} %param.34) | copy-start | bytes 12292
  6.5 10.5 %copy-start.7 = (bf16[256,192]{0,1:T(8,128)(2,1)S(1)}, bf16[256,192]{0,1:T(8,128)(2,1)}, u32[]{:S(2)}) copy-start(bf16[256,192]{0,1:T(8,128)(2,1)} %param.24) | copy-start | bytes 294916
  6.5 125.6 %all-to-all-start.1 = ((bf16[4,2048,128]{2,1,0:T(8,128)(2,1)}), bf16[4,2048,128]{2,1,0:T(8,128)(2,1)}, u32[]{:S(2)}, u32[]{:S(2)}) async-start(bf16[4,2048,128]{2,1,0:T(8,128)(2,1)} %param.36), calls=%async_computation.1 | async-start | bytes 4194304 | tf_op jit(solution)/shard_map/all_to_all | solution.py:147
  11.3 77.7 %copy-start.5 = (pred[256,256]{1,0:T(8,128)(4,1)}, pred[256,256]{1,0:T(8,128)(4,1)S(1)}, u32[]{:S(2)}) copy-start(pred[256,256]{1,0:T(8,128)(4,1)S(1)} %iota_compare_fusion) | copy-start | bytes 196612
  15.6 1.0 copy-start.16
  16.5 0.5 copy-start.15
  18.2 70.9 %copy-start.9 = (s32[8,128]{1,0:T(8,128)S(1)}, s32[8,128]{1,0:T(8,128)}, u32[]{:S(2)}) copy-start(s32[8,128]{1,0:T(8,128)} %eq.28) | copy-start | bytes 12292
  18.2 90.7 %copy-start.13 = (f32[2,256]{1,0:T(2,128)S(1)}, f32[2,256]{1,0:T(2,128)}, u32[]{:S(2)}) copy-start(f32[2,256]{1,0:T(2,128)} %param.26) | copy-start | bytes 6148
  108.1 12.6 %copy-start.8 = (bf16[256,192]{0,1:T(8,128)(2,1)S(1)}, bf16[256,192]{0,1:T(8,128)(2,1)}, u32[]{:S(2)}) copy-start(bf16[256,192]{0,1:T(8,128)(2,1)} %param.25) | copy-start | bytes 294916
  132.1 4.6 %copy-start.12 = (f32[2048]{0:T(1024)S(1)}, f32[2048]{0:T(1024)}, u32[]{:S(2)}) copy-start(f32[2048]{0:T(1024)} %param.33) | copy-start | bytes 24580
  132.1 30.3 %all-to-all-start.2 = ((bf16[4,2048,128]{2,1,0:T(8,128)(2,1)}), bf16[4,2048,128]{2,1,0:T(8,128)(2,1)}, u32[]{:S(2)}, u32[]{:S(2)}) async-start(bf16[4,2048,128]{2,1,0:T(8,128)(2,1)} %param.37), calls=%async_computation.2 | async-start | bytes 4194304 | tf_op jit(solution)/shard_map/all_to_all | solution.py:148
  138.5 1.1 copy-start.1
  215.0 30.2 %all-to-all-start.3 = ((bf16[4,128,2048]{2,1,0:T(8,128)(2,1)}), bf16[4,128,2048]{2,1,0:T(8,128)(2,1)}, u32[]{:S(2)}, u32[]{:S(2)}) async-start(bf16[4,128,2048]{2,1,0:T(8,128)(2,1)} %param.38), calls=%async_computation.3 | async-start | bytes 4194304 | tf_op jit(solution)/shard_map/all_to_all | solution.py:150
  237.1 3.6 copy-start.2
  237.2 3.6 copy-start.3
  245.2 1.9 copy-start.4
  254.1 4.9 %copy-start.11 = (s32[256,4]{0,1:T(4,128)S(1)}, s32[256,4]{0,1:T(4,128)}, u32[]{:S(2)}) copy-start(s32[256,4]{0,1:T(4,128)} %param.34) | copy-start | bytes 12292
  254.1 5.7 %copy-start.14 = (f32[256,4]{0,1:T(4,128)S(1)}, f32[256,4]{0,1:T(4,128)}, u32[]{:S(2)}) copy-start(f32[256,4]{0,1:T(4,128)} %param.35) | copy-start | bytes 12292
  254.1 52.7 %all-to-all-start.4 = ((bf16[8,1,64,2048]{3,2,1,0:T(8,128)(2,1)}), bf16[8,1,64,2048]{3,2,1,0:T(8,128)(2,1)}, u32[]{:S(2)}, u32[]{:S(2)}) async-start(bf16[8,1,64,2048]{3,2,1,0:T(8,128)(2,1)} %fusion.5), calls=%async_computation.4 | async-start | bytes 4194304 | tf_op jit(solution)/shard_map/all_to_all | solution.py:174
  258.6 104.5 %reduce-scatter.2.cloned.1.call-start = ((), (), s32[]{:S(2)}) async-start(), calls=%async_computation.6 | async-start | bytes 1310720 | tf_op jit(solution)/shard_map/reduce_scatter | solution.py:188
  317.5 7.2 %copy-start.6 = (pred[256,4]{1,0:T(8,128)(4,1)S(1)}, pred[256,4]{1,0:T(8,128)(4,1)}, u32[]{:S(2)}) copy-start(pred[256,4]{1,0:T(8,128)(4,1)} %compare_and_fusion) | copy-start | bytes 3076
Sparse Core Ops, SparseCore 0:
  340.1 22.8 reduce-scatter.1
where the time goes:
time: 375 us; the launch traced here: 372 us
  blocking collectives  117 us (31%)
  waiting for transfers between devices  79.9 us (21%)
  local copies, waits for them, and re-layouts  57.7 us (15%)
  other arithmetic  54.8 us (15%)
  matrix products  29.4 us (8%)
  starting transfers between devices  18.7 us (5%)
  between operations  14.3 us (4%)
    all_to_all x1, blocking collectives, body(): lax.all_to_all(outgoing, 'sp', split_axis=0, concat_axis=0, tiled=True)  52.6 us
    all_to_all x1, waiting for transfers between devices, body(): lax.all_to_all(expert_rows, 'sp', split_axis=0, concat_axis=0, tiled=True)  42.7 us
    all_gather x1, blocking collectives, entering(): everything = jax.tree.map(lambda part: lax.all_gather(part, axis), shard)  35.5 us
    reduce_scatter x1, waiting for transfers between devices, body(): lax.psum_scatter((routed_partial + shared_rounded).astype(jnp.bfloat16),...  23 us
    unnamed x1, blocking collectives  21.7 us
    gather x2, local copies, waits for them, and re-layouts, body(): jnp.take(back_flat, local_position, axis=0)  17.9 us
    another operation x5, other arithmetic  17.9 us
    all_to_all x1, waiting for transfers between devices, body(): lax.all_to_all(routed_up_weight, 'tp', split_axis=0, concat_axis=2, tiled...  11.9 us
  transfers between devices with their start and end apart: 5, of which 4 were waited for; matrix products, arithmetic and copies ran while one was open for 26% of the time, Pallas kernels for 0%

commit v1 on v0

v1 whole, which is shorter than its diff:
```python
import jax
import jax.numpy as jnp
from jax import lax
from jax.experimental import pallas as pl
from jax.experimental.pallas import tpu as pltpu
from jax.sharding import PartitionSpec as P

NEG_LARGE = -1e30
EPSILON = 1e-06


def spreads(experts_total, top_count):
    return experts_total <= 16 * top_count


def entering(local_memory, local_top, ending, routes, router_weight_matrix):
    count, here = (lax.axis_size("sp"), lax.axis_index("sp"))
    heads_here, head_size, _ = local_memory.shape
    top_count = routes.shape[1]
    lanes = -(-head_size // 128) * 128
    rows = heads_here * head_size
    memory_rows = jnp.pad(local_memory.reshape(rows, head_size), ((0, 0), (0, lanes - head_size)))
    logs = jnp.pad(jnp.stack([local_top, ending]), ((0, 6), (0, lanes - heads_here)))
    routing = jnp.concatenate([routes.astype(jnp.float32).T, router_weight_matrix.T], axis=0)
    packed = jnp.concatenate([memory_rows, logs, routing.reshape(-1, lanes)], axis=0)
    everything = lax.all_gather(packed, "sp")
    memories = everything[:, :rows, :head_size].reshape(count, heads_here, head_size, head_size)
    tops = everything[:, rows, :heads_here]
    totals = everything[:, rows + 1, :heads_here]
    routing_all = everything[:, rows + 8 :].reshape(count, 2 * top_count, -1)
    block = jnp.arange(count, dtype=jnp.int32)
    between = (block[None, :] > block[:, None]) & (block[None, :] < here)
    later = jnp.sum(jnp.where(between[:, :, None], totals[None], 0.0), axis=1)
    reached = (block < here)[:, None]
    logs_all = jnp.where(reached, tops + later, NEG_LARGE)
    stabil = jnp.max(logs_all, axis=0)
    share = jnp.where(reached, jnp.exp(logs_all - stabil[None]), 0.0)
    memory = jnp.sum(share[:, :, None, None] * memories, axis=0)
    return memory, stabil, routing_all[:, :top_count], routing_all[:, top_count:]


def experts_kernel(
    here_ref, x_ref, weight_ref, gate_ref, up_ref, down_ref,
    shared_gate_ref, shared_up_ref, shared_down_ref, out_ref, both_ref, hidden_ref,
):
    block = pl.program_id(0)
    experts, _, width = gate_ref.shape
    pieces, out_width = out_ref.shape[1], out_ref.shape[3]

    @pl.when(block == 0)
    def _():
        for e in range(experts):
            both_ref[e, :, :width] = gate_ref[e]
            both_ref[e, :, width:] = up_ref[e]
        both_ref[experts, :, :width] = shared_gate_ref[...]
        both_ref[experts, :, width:] = shared_up_ref[...]

    def hidden_of(e):
        both = jnp.dot(x_ref[...], both_ref[e], preferred_element_type=jnp.float32)
        return jax.nn.silu(both[:, :width]) * both[:, width:]

    for e in range(experts):
        hidden_ref[:, e * width : (e + 1) * width] = (
            hidden_of(e) * weight_ref[:, e : e + 1]
        ).astype(jnp.bfloat16)

    def piece_of(j):
        columns = slice(j * out_width, (j + 1) * out_width)
        total = jnp.dot(
            hidden_ref[:, :width], down_ref[0, :, columns], preferred_element_type=jnp.float32
        )
        for e in range(1, experts):
            total += jnp.dot(
                hidden_ref[:, e * width : (e + 1) * width],
                down_ref[e, :, columns],
                preferred_element_type=jnp.float32,
            )
        return total

    @pl.when(block == here_ref[0])
    def _():
        shared_hidden = hidden_of(experts).astype(jnp.bfloat16)
        for j in range(pieces):
            columns = slice(j * out_width, (j + 1) * out_width)
            out_ref[0, j] = (
                piece_of(j)
                + jnp.dot(
                    shared_hidden, shared_down_ref[:, columns], preferred_element_type=jnp.float32
                )
            ).astype(jnp.bfloat16)

    @pl.when(block != here_ref[0])
    def _():
        for j in range(pieces):
            out_ref[0, j] = piece_of(j).astype(jnp.bfloat16)


def spread_experts(
    stream,
    normed,
    all_routes,
    all_weights,
    routed_gate_weight,
    routed_up_weight,
    routed_down_weight,
    shared_gate_weight,
    shared_up_weight,
    shared_down_weight,
):
    tokens_here, model_width = normed.shape
    sp_count, tp_count = (lax.axis_size("sp"), lax.axis_size("tp"))
    sp_index, tp_index = (lax.axis_index("sp"), lax.axis_index("tp"))
    local_experts, _, width = routed_gate_weight.shape
    part = tokens_here // tp_count
    width_share = model_width // tp_count
    mine = lax.dynamic_slice_in_dim(normed, tp_index * part, part, 0)
    rows = lax.all_gather(mine, ("sp", "tp"), axis=0, tiled=True)
    first = (sp_index * local_experts).astype(jnp.float32)
    named = first + jnp.arange(local_experts, dtype=jnp.float32)
    weight = jnp.sum(
        jnp.where(all_routes[:, :, None, :] == named[None, None, :, None], all_weights[:, :, None, :], 0.0),
        axis=1,
    )
    weight = weight.transpose(0, 2, 1).reshape(sp_count * tokens_here, local_experts)
    whole = lambda *shape: pl.BlockSpec(shape, lambda b, here: (0,) * len(shape))
    partial = pl.pallas_call(
        experts_kernel,
        out_shape=jax.ShapeDtypeStruct((sp_count, tp_count, tokens_here, width_share), jnp.bfloat16),
        grid_spec=pltpu.PrefetchScalarGridSpec(
            num_scalar_prefetch=1,
            grid=(sp_count,),
            in_specs=[
                pl.BlockSpec((tokens_here, model_width), lambda b, here: (b, 0)),
                pl.BlockSpec((tokens_here, local_experts), lambda b, here: (b, 0)),
                whole(*routed_gate_weight.shape),
                whole(*routed_up_weight.shape),
                whole(*routed_down_weight.shape),
                whole(*shared_gate_weight.shape),
                whole(*shared_up_weight.shape),
                whole(*shared_down_weight.shape),
            ],
            out_specs=pl.BlockSpec(
                (1, tp_count, tokens_here, width_share), lambda b, here: (b, 0, 0, 0)
            ),
            scratch_shapes=[
                pltpu.VMEM((local_experts + 1, model_width, 2 * width), jnp.bfloat16),
                pltpu.VMEM((tokens_here, local_experts * width), jnp.bfloat16),
            ],
        ),
        compiler_params=pltpu.CompilerParams(dimension_semantics=("arbitrary",)),
    )(
        sp_index.astype(jnp.int32).reshape(1),
        rows,
        weight,
        routed_gate_weight,
        routed_up_weight,
        routed_down_weight,
        shared_gate_weight,
        shared_up_weight,
        shared_down_weight,
    )
    combined = lax.psum_scatter(
        partial.reshape(sp_count * tp_count, tokens_here, width_share),
        ("sp", "tp"),
        scatter_dimension=0,
        tiled=True,
    ).reshape(tokens_here, width_share)
    stream_share = lax.dynamic_slice_in_dim(stream, tp_index * width_share, width_share, 1)
    return (stream_share + combined.astype(jnp.float32)).astype(jnp.bfloat16)


def exchange_experts(
    stream,
    normed,
    routes,
    router_weight_matrix,
    routed_gate_weight,
    routed_up_weight,
    routed_down_weight,
    shared_gate_weight,
    shared_up_weight,
    shared_down_weight,
):
    tokens_here, model_width = normed.shape
    sp_count = lax.axis_size("sp")
    tp_count = lax.axis_size("tp")
    tp_index = lax.axis_index("tp")
    local_experts = routed_gate_weight.shape[0]
    experts_total = local_experts * sp_count
    top_count = routes.shape[1]
    capacity = 2 * tokens_here * top_count // experts_total
    width_share = model_width // tp_count
    flat_routes = routes.reshape(-1)
    onehot = (flat_routes[:, None] == jnp.arange(experts_total, dtype=jnp.int32)[None, :]).astype(
        jnp.int32
    )
    earlier_count = jnp.cumsum(onehot, axis=0) - onehot
    slot_index = jnp.sum(earlier_count * onehot, axis=1)
    position = flat_routes * capacity + slot_index
    owner = jnp.arange(flat_routes.shape[0], dtype=jnp.int32) // top_count
    slot_token = (
        jnp.full((experts_total * capacity,), tokens_here, jnp.int32).at[position].set(owner)
    )
    padded = jnp.concatenate([normed, jnp.zeros((1, model_width), jnp.bfloat16)], axis=0)
    shared_hidden = (
        jax.nn.silu(jnp.dot(normed, shared_gate_weight, preferred_element_type=jnp.float32))
        * jnp.dot(normed, shared_up_weight, preferred_element_type=jnp.float32)
    ).astype(jnp.bfloat16)
    shared_partial = jnp.dot(shared_hidden, shared_down_weight, preferred_element_type=jnp.float32)
    stream_share = lax.dynamic_slice_in_dim(stream, tp_index * width_share, width_share, 1)
    group_count = local_experts // tp_count
    whole_gate, whole_up = (
        lax.all_to_all(routed_gate_weight, "tp", split_axis=0, concat_axis=2, tiled=True),
        lax.all_to_all(routed_up_weight, "tp", split_axis=0, concat_axis=2, tiled=True),
    )
    whole_down = lax.all_to_all(routed_down_weight, "tp", split_axis=0, concat_axis=1, tiled=True)
    slot_table = slot_token.reshape(sp_count, local_experts, capacity)
    chosen = lax.dynamic_slice_in_dim(slot_table, tp_index * group_count, group_count, 1)
    outgoing = jnp.take(padded, chosen.reshape(-1), axis=0).reshape(
        sp_count, group_count, capacity, model_width
    )
    arrived = lax.all_to_all(outgoing, "sp", split_axis=0, concat_axis=0, tiled=True)
    gate_vals = jnp.einsum(
        "secd,edf->secf", arrived, whole_gate, preferred_element_type=jnp.float32
    )
    up_vals = jnp.einsum("secd,edf->secf", arrived, whole_up, preferred_element_type=jnp.float32)
    expert_hidden = (jax.nn.silu(gate_vals) * up_vals).astype(jnp.bfloat16)
    hidden_width = whole_down.shape[1]
    group_width = hidden_width // tp_count
    expert_sum = jnp.zeros(arrived.shape[:3] + (model_width,), jnp.float32)
    for index in range(tp_count):
        piece = jnp.einsum(
            "secf,efd->secd",
            expert_hidden[..., index * group_width : (index + 1) * group_width],
            whole_down[:, index * group_width : (index + 1) * group_width, :],
            preferred_element_type=jnp.float32,
        )
        expert_sum = expert_sum + piece.astype(jnp.bfloat16).astype(jnp.float32)
    expert_rows = expert_sum.astype(jnp.bfloat16)
    back = lax.all_to_all(expert_rows, "sp", split_axis=0, concat_axis=0, tiled=True)
    back_flat = back.reshape(sp_count * group_count * capacity, model_width)
    owner_sp = flat_routes // local_experts
    local_slot = flat_routes % local_experts - tp_index * group_count
    belongs = (local_slot >= 0) & (local_slot < group_count)
    local_position = jnp.where(
        belongs, (owner_sp * group_count + local_slot) * capacity + slot_index, 0
    )
    picked = jnp.take(back_flat, local_position, axis=0).reshape(
        tokens_here, top_count, model_width
    )
    kept_weight = jnp.where(belongs.reshape(tokens_here, top_count), router_weight_matrix, 0.0)
    routed_partial = jnp.sum(kept_weight[:, :, None] * picked.astype(jnp.float32), axis=1)
    shared_rounded = shared_partial.astype(jnp.bfloat16).astype(jnp.float32)
    combined = lax.psum_scatter(
        (routed_partial + shared_rounded).astype(jnp.bfloat16),
        "tp",
        scatter_dimension=1,
        tiled=True,
    ).astype(jnp.float32)
    return (stream_share + combined).astype(jnp.bfloat16)


def body(
    memory_queries,
    memory_keys,
    memory_values,
    output_gate_preactivation,
    log_input_gate,
    forget_preactivation,
    head_forget_bias,
    forget_extra_boost,
    head_norm_gain,
    memory_output_weight,
    residual,
    expert_norm_gain,
    routes,
    router_weight_matrix,
    routed_gate_weight,
    routed_up_weight,
    routed_down_weight,
    shared_gate_weight,
    shared_up_weight,
    shared_down_weight,
):
    tokens_here = memory_queries.shape[0]
    heads_here = log_input_gate.shape[0]
    head_size = memory_queries.shape[1] // heads_here
    scale = head_size ** (-0.5)
    queries = memory_queries.reshape(tokens_here, heads_here, head_size)
    keyset = memory_keys.reshape(tokens_here, heads_here, head_size)
    valueset = memory_values.reshape(tokens_here, heads_here, head_size)
    forget_log_gate = (
        jax.nn.log_sigmoid(forget_preactivation + head_forget_bias[:, None]) + forget_extra_boost
    )
    cumul = jnp.cumsum(forget_log_gate, axis=1)
    causal = jnp.tril(jnp.ones((tokens_here, tokens_here), bool))
    d_log = jnp.where(
        causal[None], cumul[:, :, None] - cumul[:, None, :] + log_input_gate[:, None, :], NEG_LARGE
    )
    ending = cumul[:, -1]
    w_log = ending[:, None] - cumul + log_input_gate
    local_top = jnp.max(w_log, axis=1)
    w_end = jnp.exp(w_log - local_top[:, None])
    keys_float = keyset.astype(jnp.float32)
    values_float = valueset.astype(jnp.float32)
    local_memory = jnp.einsum(
        "hs,shd,she->hde", w_end, keys_float, values_float, precision=lax.Precision.HIGHEST
    )
    memory, stabil, all_routes, all_weights = entering(
        local_memory, local_top, ending, routes, router_weight_matrix
    )
    g_log = cumul + stabil[:, None]
    top = jnp.maximum(g_log, jnp.max(d_log, axis=2))
    scores = jnp.einsum("thd,shd->hts", queries, keyset, preferred_element_type=jnp.float32) * scale
    weights = scores * jnp.exp(d_log - top[:, :, None])
    inter = jnp.exp(g_log - top)
    q_scaled = queries.astype(jnp.float32) * scale
    numer = jnp.einsum(
        "hts,shd->thd", weights.astype(jnp.bfloat16), valueset, preferred_element_type=jnp.float32
    )
    hidden = numer + inter.T[:, :, None] * jnp.einsum(
        "thd,hde->the", q_scaled, memory, precision=lax.Precision.HIGHEST
    )
    hidden = hidden * lax.rsqrt(jnp.mean(hidden * hidden, axis=2, keepdims=True) + EPSILON)
    token_mixing = (
        hidden.reshape(tokens_here, heads_here * head_size)
        * head_norm_gain
        * jax.nn.sigmoid(output_gate_preactivation.astype(jnp.float32))
    ).astype(jnp.bfloat16)
    mixed = jnp.dot(
        lax.all_gather(token_mixing, "tp", axis=1, tiled=True),
        memory_output_weight,
        preferred_element_type=jnp.float32,
    )
    stream = residual.astype(jnp.float32) + mixed
    normed = (
        stream
        * lax.rsqrt(jnp.mean(stream * stream, axis=1, keepdims=True) + EPSILON)
        * expert_norm_gain
    ).astype(jnp.bfloat16)
    weights_here = (
        routed_gate_weight,
        routed_up_weight,
        routed_down_weight,
        shared_gate_weight,
        shared_up_weight,
        shared_down_weight,
    )
    experts_total = routed_gate_weight.shape[0] * lax.axis_size("sp")
    if spreads(experts_total, routes.shape[1]):
        return spread_experts(stream, normed, all_routes, all_weights, *weights_here)
    return exchange_experts(stream, normed, routes, router_weight_matrix, *weights_here)


def solution(mesh):
    in_specs = (
        P("sp", "tp"),
        P("sp", "tp"),
        P("sp", "tp"),
        P("sp", "tp"),
        P("tp", "sp"),
        P("tp", "sp"),
        P("tp"),
        P("tp", "sp"),
        P("tp"),
        P(),
        P("sp", None),
        P(),
        P("sp", None),
        P("sp", None),
        P("sp", None, "tp"),
        P("sp", None, "tp"),
        P("sp", "tp", None),
        P(None, "tp"),
        P(None, "tp"),
        P("tp", None),
    )
    out_specs = P("sp", "tp")
    return jax.shard_map(body, mesh=mesh, in_specs=in_specs, out_specs=out_specs, check_vma=False)
```

time: 375 us -> 327 us (0.87)
  waiting for transfers between devices: 79.9 us -> 224 us
  blocking collectives: 117 us -> 40.5 us
  local copies, waits for them, and re-layouts: 57.7 us -> 4.11 us
  other arithmetic: 54.8 us -> 11.8 us
  Pallas kernels: 0 us -> 26.2 us
  matrix products: 29.4 us -> 6.41 us
  starting transfers between devices: 18.7 us -> 0.04 us
    reduce_scatter x1, waiting for transfers between devices: 23 us -> 149 us  [spread_experts(): lax.psum_scatter(partial.reshape(sp_count * tp_count, tokens_here, width_...]
    all_gather x0 -> x1, waiting for transfers between devices: none -> 75.4 us  [spread_experts(): rows = lax.all_gather(mine, ('sp', 'tp'), axis=0, tiled=True)]
    all_to_all x4 -> x0, waiting for transfers between devices: 56.8 us -> none  [the longest x1 42.7 us: body(): lax.all_to_all(expert_rows, 'sp', split_axis=0, concat_axis=0, tiled=True)]
    all_to_all x1 -> x0, blocking collectives: 52.6 us -> none  [body(): lax.all_to_all(outgoing, 'sp', split_axis=0, concat_axis=0, tiled=True)]
    pallas_call x0 -> x1, Pallas kernels: none -> 26.2 us  [spread_experts(): pl.pallas_call(experts_kernel, out_shape=jax.ShapeDtypeStruct((sp_count,...]
    gather x3 -> x0, local copies, waits for them, and re-layouts: 24.5 us -> none  [the longest x2 17.9 us: body(): jnp.take(back_flat, local_position, axis=0)]
    unnamed x1 -> x0, blocking collectives: 21.7 us -> none
    dot_general x8 -> x0, matrix products: 20.4 us -> none  [the longest x4 8.88 us: body(): jnp.einsum('secf,efd->secd', expert_hidden[..., index * group_width:(inde...]
  transfers between devices with their start and end apart: 5 -> 2, of which waited for: 4 -> 2; matrix products, arithmetic and copies ran while one was open for 26% -> 1% of each run, Pallas kernels for 0% -> 0%
where the time goes in v1:
time: 327 us
  waiting for transfers between devices  224 us (69%)
  blocking collectives  40.5 us (12%)
  Pallas kernels  26.2 us (8%)
  between operations  13.6 us (4%)
  other arithmetic  11.8 us (4%)
  matrix products  6.41 us (2%)
  local copies, waits for them, and re-layouts  4.11 us (1%)
    reduce_scatter x1, waiting for transfers between devices, spread_experts(): lax.psum_scatter(partial.reshape(sp_count * tp_count, tokens_here, width_...  149 us
    all_gather x1, waiting for transfers between devices, spread_experts(): rows = lax.all_gather(mine, ('sp', 'tp'), axis=0, tiled=True)  75.4 us
    all_gather x1, blocking collectives, entering(): everything = lax.all_gather(packed, 'sp')  34.1 us
    pallas_call x1, Pallas kernels, spread_experts(): pl.pallas_call(experts_kernel, out_shape=jax.ShapeDtypeStruct((sp_count,...  26.2 us
  transfers between devices with their start and end apart: 2, of which 2 were waited for; matrix products, arithmetic and copies ran while one was open for 1% of the time, Pallas kernels for 0%

profile of v1, /device:TPU:0, one launch (start us, length us, event | category | flops | bytes accessed | tf_op | source)
XLA Modules:
  0.0 326.9 jit_solution(8225829800345570274)
XLA Ops:
  6.5 0.0 copy-start
  6.5 0.0 copy-start.4
  6.5 0.0 all-gather.3.cloned.1.call-start
  6.6 0.9 fusion.32
  7.6 0.6 reduce-window.6
  8.2 0.2 slice_reduce_fusion
  8.3 0.2 reduce-window.9
  8.5 0.1 add_bitcast_fusion
  8.6 0.2 slice_reduce_fusion.1
  8.8 0.7 convert_bitcast_fusion
  9.5 0.7 pad_maximum_fusion
  10.2 0.9 fusion.38
  11.0 0.9 fusion.12
  12.0 0.1 exponential_bitcast_fusion.1
  12.1 1.2 fusion.24
  13.3 0.0 copy-start.5
  13.3 34.1 %all-gather = f32[1728,128]{1,0:T(8,128)S(1)} all-gather(f32[216,128]{1,0:T(8,128)S(1)} %fusion.27), channel_id=2, replica_groups=mesh['sp'=8,'tp'=4] {'sp'}, dimensions={0}, use_global_device_ids=true | all-gather | bytes 995328 | tf_op jit(solution)/shard_map/all_gather | solution.py:26
  47.4 0.0 copy-start.1
  47.4 1.0 copy-done.1
  48.3 0.1 copy.29
  48.4 0.1 copy.30
  48.5 0.1 select_reduce_fusion.1
  48.6 0.1 fusion.34
  48.7 0.1 exponential_select_fusion
  48.8 0.1 exponential_bitcast_fusion
  48.9 0.1 copy.31
  48.9 0.1 mul.90
  49.0 0.1 mul.91
  49.1 1.4 fusion.6
  50.5 0.0 copy-done.4
  50.5 1.5 fusion.5
  52.0 0.0 copy-start.2
  52.0 1.4 multiply_reduce_fusion.1
  53.5 0.0 copy-done.5
  53.5 1.0 fusion.21
  54.5 6.5 %all_gather.14 = bf16[256,768]{0,1:T(8,128)(2,1)S(1)} all-gather(bf16[256,192]{0,1:T(8,128)(2,1)S(1)} %fusion.21), channel_id=1, replica_groups=mesh['sp'=8,'tp'=4] {'tp'}, dimensions={1}, use_global_device_ids=true | all-gather | bytes 491520 | tf_op jit(solution)/shard_map/all_gather | solution.py:331
  60.9 0.0 copy-done
  60.9 0.0 copy-done.2
  60.9 0.0 copy-start.3
  60.9 2.4 multiply_reduce_fusion
  63.3 0.1 dynamic-slice
  63.4 0.0 copy-done.3
  63.4 1.9 fusion.8
  65.3 0.0 all-gather.3.cloned.1.call-update
  65.3 0.0 reduce-scatter.2.cloned.1.call-start
  65.3 0.9 slice.41
  66.3 0.1 select_reduce_fusion
  66.4 1.4 copy.35
  67.7 75.4 %all-gather.3.cloned.1.call-done.x_ref = bf16[2048,2048]{1,0:T(8,128)(2,1)} async-done(((bf16[64,2048]{1,0:T(8,128)(2,1)}), bf16[2048,2048]{1,0:T(8,128)(2,1)}) %all-gather.3.cloned.1.call-update) | async-done | bytes 8388624 | tf_op jit(solution)/shard_map/all_gather | solution.py:117
  143.1 26.2 %shard_map.190 = bf16[8,4,256,512]{3,2,1,0:T(8,128)(2,1)} custom-call(s32[1]{0:T(128)} %bitcast.16.here_ref, bf16[2048,2048]{1,0:T(8,128)(2,1)} %all-gather.3.cloned.1.call-done.x_ref, f32[2048,4]{1,0:T(8,128)} %bitcast.68, bf16[4,2048,128]{2,1,0:T(8,128)(2,1)} %gate_ref.1, bf16[4,2048,128]{2,1,0:T(8,128)(2,1)} %up_ref.1, bf16[4,128,2048]{2,1,0:T(8,128)(2,1)} %down_ref.1, ...), custom_call_target="tpu_custom_call" | custom-call | tf_op jit(solution)/shard_map/pallas_call | solution.py:126
  169.3 0.0 reduce-scatter.2.cloned.1.call-update
  169.3 148.9 %reduce-scatter.2.cloned.1.call-done = bf16[1,256,512]{2,1,0:T(8,128)(2,1)} async-done(((bf16[32,256,512]{2,1,0:T(8,128)(2,1)}), bf16[1,256,512]{2,1,0:T(8,128)(2,1)}) %reduce-scatter.2.cloned.1.call-update) | async-done | bytes 262160 | tf_op jit(solution)/shard_map/reduce_scatter | solution.py:162
  318.2 1.9 fusion.9
  (17 shorter events, 0.2 us)
Async XLA Ops:
  6.5 54.4 %copy-start = (bf16[768,2048]{1,0:T(8,128)(2,1)S(1)}, bf16[768,2048]{1,0:T(8,128)(2,1)}, u32[]{:S(2)}) copy-start(bf16[768,2048]{1,0:T(8,128)(2,1)} %param.29) | copy-start | bytes 9437188
  6.5 44.0 %copy-start.4 = (f32[2,256]{1,0:T(2,128)S(1)}, f32[2,256]{1,0:T(2,128)}, u32[]{:S(2)}) copy-start(f32[2,256]{1,0:T(2,128)} %param.24) | copy-start | bytes 6148
  6.5 136.5 %all-gather.3.cloned.1.call-start = ((), (), s32[]{:S(2)}) async-start(), calls=%async_computation.1 | async-start | bytes 8650752 | tf_op jit(solution)/shard_map/all_gather | solution.py:117
  13.3 40.2 %copy-start.5 = (f32[192]{0:T(256)S(1)}, f32[192]{0:T(256)}, u32[]{:S(2)}) copy-start(f32[192]{0:T(256)} %param.28) | copy-start | bytes 2308
  47.4 1.0 copy-start.1
  52.0 8.9 %copy-start.2 = (bf16[256,2048]{1,0:T(8,128)(2,1)S(1)}, bf16[256,2048]{1,0:T(8,128)(2,1)}, u32[]{:S(2)}) copy-start(bf16[256,2048]{1,0:T(8,128)(2,1)} %param.30) | copy-start | bytes 3145732
  60.9 2.5 copy-start.3
  65.3 252.9 %reduce-scatter.2.cloned.1.call-start = ((), (), s32[]{:S(2)}) async-start(), calls=%async_computation.2 | async-start | bytes 8650752 | tf_op jit(solution)/shard_map/reduce_scatter | solution.py:162
Sparse Core Ops, SparseCore 0:
  65.4 77.6 all-gather.2
  169.4 148.7 reduce-scatter.1

commit v2 on v1

--- a/solution.py
+++ b/solution.py
@@ -9,8 +9,8 @@
 EPSILON = 1e-06
 
 
-def spreads(experts_total, top_count):
-    return experts_total <= 16 * top_count
+def spreads(experts_total, top_count, tp_count):
+    return experts_total <= 16 * top_count and tp_count == 4
 
 
 def entering(local_memory, local_top, ending, routes, router_weight_matrix):
@@ -93,6 +93,48 @@
     def _():
         for j in range(pieces):
             out_ref[0, j] = piece_of(j).astype(jnp.bfloat16)
+
+
+def ring_order(count):
+    return list(range(0, count, 2)) + list(range(count - 1, 0, -2))
+
+
+def add_rounded(a, b):
+    return (a.astype(jnp.float32) + b.astype(jnp.float32)).astype(jnp.bfloat16)
+
+
+def reduce_scatter(partial):
+    sp_count, tp_count, tokens, width = partial.shape
+    sp_index, tp_index = (lax.axis_index("sp"), lax.axis_index("tp"))
+    near, far = tp_index % 2, tp_index // 2
+    pairs = partial.reshape(sp_count, tp_count // 2, 2, tokens, width)
+    swap_near = [(i, i ^ 1) for i in range(tp_count)]
+    given = lax.dynamic_index_in_dim(pairs, 1 - near, 2, keepdims=False)
+    kept = lax.dynamic_index_in_dim(pairs, near, 2, keepdims=False)
+    kept = add_rounded(kept, lax.ppermute(given, "tp", swap_near))
+
+    order = ring_order(sp_count)
+    place_of = [order.index(i) for i in range(sp_count)]
+    place = jnp.asarray(place_of, jnp.int32)[sp_index]
+    order_array = jnp.asarray(order, jnp.int32)
+    half = tokens // 2
+    sums = []
+    for turn, rows in ((1, slice(0, half)), (-1, slice(half, tokens))):
+        links = [(order[p], order[(p + turn) % sp_count]) for p in range(sp_count)]
+
+        def block(k):
+            owner = order_array[(place - turn * k) % sp_count]
+            return lax.dynamic_index_in_dim(kept[:, :, rows], owner, 0, keepdims=False)
+
+        moving = block(1)
+        for k in range(2, sp_count + 1):
+            moving = add_rounded(lax.ppermute(moving, "sp", links), block(k))
+        sums.append(moving)
+    mine = jnp.concatenate(sums, axis=1)
+    swap_far = [(i, (i + 2) % tp_count) for i in range(tp_count)]
+    given = lax.dynamic_index_in_dim(mine, 1 - far, 0, keepdims=False)
+    kept = lax.dynamic_index_in_dim(mine, far, 0, keepdims=False)
+    return kept.astype(jnp.float32) + lax.ppermute(given, "tp", swap_far).astype(jnp.float32)
 
 
 def spread_experts(
@@ -159,12 +201,7 @@
         shared_up_weight,
         shared_down_weight,
     )
-    combined = lax.psum_scatter(
-        partial.reshape(sp_count * tp_count, tokens_here, width_share),
-        ("sp", "tp"),
-        scatter_dimension=0,
-        tiled=True,
-    ).reshape(tokens_here, width_share)
+    combined = reduce_scatter(partial)
     stream_share = lax.dynamic_slice_in_dim(stream, tp_index * width_share, width_share, 1)
     return (stream_share + combined.astype(jnp.float32)).astype(jnp.bfloat16)
 
@@ -347,7 +384,7 @@
         shared_down_weight,
     )
     experts_total = routed_gate_weight.shape[0] * lax.axis_size("sp")
-    if spreads(experts_total, routes.shape[1]):
+    if spreads(experts_total, routes.shape[1], lax.axis_size("tp")):
         return spread_experts(stream, normed, all_routes, all_weights, *weights_here)
     return exchange_experts(stream, normed, routes, router_weight_matrix, *weights_here)
 

time: 327 us -> 283 us (0.87)
  waiting for transfers between devices: 224 us -> 84.5 us
  between operations: 13.6 us -> 54.4 us
  other arithmetic: 11.8 us -> 36.9 us
  starting transfers between devices: 0.04 us -> 16.2 us
  local copies, waits for them, and re-layouts: 4.11 us -> 15.3 us
    reduce_scatter x1 -> x0, waiting for transfers between devices: 149 us -> none  [spread_experts(): lax.psum_scatter(partial.reshape(sp_count * tp_count, tokens_here, width_...]
    convert_element_type x0 -> x15, other arithmetic: none -> 24.4 us  [add_rounded(): return (a.astype(jnp.float32) + b.astype(jnp.float32)).astype(jnp.bfloat16)]
    ppermute x0 -> x16, starting transfers between devices: none -> 16.2 us  [the longest x14 14.5 us: reduce_scatter(): moving = add_rounded(lax.ppermute(moving, 'sp', links), block(k))]
    ppermute x0 -> x16, waiting for transfers between devices: none -> 9.15 us  [the longest x1 5.27 us: reduce_scatter(): lax.ppermute(given, 'tp', swap_far).astype(jnp.float32)]
    squeeze x0 -> x3, local copies, waits for them, and re-layouts: none -> 6.23 us  [the longest x1 4.54 us: reduce_scatter(): given = lax.dynamic_index_in_dim(pairs, 1 - near, 2, keepdims=False)]
  transfers between devices with their start and end apart: 2 -> 17, of which waited for: 2 -> 5; matrix products, arithmetic and copies ran while one was open for 1% -> 8% of each run, Pallas kernels for 0% -> 0%
where the time goes in v2:
time: 283 us; the launch traced here: 282 us
  waiting for transfers between devices  84.5 us (30%)
  between operations  54.4 us (19%)
  blocking collectives  40.6 us (14%)
  other arithmetic  36.9 us (13%)
  Pallas kernels  26.2 us (9%)
  starting transfers between devices  16.2 us (6%)
  local copies, waits for them, and re-layouts  15.3 us (5%)
  matrix products  7.53 us (3%)
    all_gather x1, waiting for transfers between devices, spread_experts(): rows = lax.all_gather(mine, ('sp', 'tp'), axis=0, tiled=True)  75.3 us
    all_gather x1, blocking collectives, entering(): everything = lax.all_gather(packed, 'sp')  34.1 us
    pallas_call x1, Pallas kernels, spread_experts(): pl.pallas_call(experts_kernel, out_shape=jax.ShapeDtypeStruct((sp_count,...  26.2 us
    convert_element_type x15, other arithmetic, add_rounded(): return (a.astype(jnp.float32) + b.astype(jnp.float32)).astype(jnp.bfloat16)  24.4 us
    ppermute x14, starting transfers between devices, reduce_scatter(): moving = add_rounded(lax.ppermute(moving, 'sp', links), block(k))  14.5 us
    all_gather x1, blocking collectives, body(): lax.all_gather(token_mixing, 'tp', axis=1, tiled=True)  6.45 us
  transfers between devices with their start and end apart: 17, of which 5 were waited for; matrix products, arithmetic and copies ran while one was open for 8% of the time, Pallas kernels for 0%

profile of v2, /device:TPU:0, one launch (start us, length us, event | category | flops | bytes accessed | tf_op | source)
XLA Modules:
  0.0 281.7 jit_solution(13032845184825159)
XLA Ops:
  6.6 0.9 fusion.52
  7.5 0.6 reduce-window.6
  8.8 0.7 convert_bitcast_fusion
  9.5 0.7 pad_maximum_fusion
  10.2 0.9 fusion.58
  11.1 1.2 fusion.44
  12.3 34.1 %all-gather = f32[1728,128]{1,0:T(8,128)S(1)} all-gather(f32[216,128]{1,0:T(8,128)S(1)} %fusion.47), channel_id=2, replica_groups=mesh['sp'=8,'tp'=4] {'sp'}, dimensions={0}, use_global_device_ids=true | all-gather | bytes 995328 | tf_op jit(solution)/shard_map/all_gather | solution.py:26
  46.4 0.9 copy-done.2
  47.6 0.9 fusion.28
  49.1 1.4 fusion.7
  50.5 1.5 fusion.6
  52.0 1.3 multiply_reduce_fusion.1
  53.3 1.0 fusion.41
  54.3 6.5 %all_gather.14 = bf16[256,768]{0,1:T(8,128)(2,1)S(1)} all-gather(bf16[256,192]{0,1:T(8,128)(2,1)S(1)} %fusion.41), channel_id=1, replica_groups=mesh['sp'=8,'tp'=4] {'tp'}, dimensions={1}, use_global_device_ids=true | all-gather | bytes 491520 | tf_op jit(solution)/shard_map/all_gather | solution.py:368
  60.8 3.6 %multiply_reduce_fusion = (f32[256]{0:T(256)S(1)}, f32[256,2048]{1,0:T(8,128)}) fusion(bf16[256,768]{0,1:T(8,128)(2,1)S(1)} %all_gather.14, bf16[768,2048]{1,0:T(8,128)(2,1)S(1)} %copy-done, bf16[256,2048]{1,0:T(8,128)(2,1)} %param.32), kind=kOutput, calls=%fused_computation.4 | convolution fusion | flops 807403264 | bytes 6685696 | tf_op jit(solution)/shard_map/dot_general | solution.py:367
  64.5 1.9 fusion.9
  66.4 0.9 slice.63
  67.4 1.4 copy.38
  68.8 75.3 %all-gather.3.cloned.1.call-done.x_ref = bf16[2048,2048]{1,0:T(8,128)(2,1)} async-done(((bf16[64,2048]{1,0:T(8,128)(2,1)}), bf16[2048,2048]{1,0:T(8,128)(2,1)}) %all-gather.3.cloned.1.call-update) | async-done | bytes 8388624 | tf_op jit(solution)/shard_map/all_gather | solution.py:159
  144.1 26.2 %shard_map.208 = bf16[8,4,256,512]{3,2,1,0:T(8,128)(2,1)} custom-call(s32[1]{0:T(128)} %bitcast.16.here_ref, bf16[2048,2048]{1,0:T(8,128)(2,1)} %all-gather.3.cloned.1.call-done.x_ref, f32[2048,4]{1,0:T(8,128)} %bitcast.158, bf16[4,2048,128]{2,1,0:T(8,128)(2,1)} %gate_ref.1, bf16[4,2048,128]{2,1,0:T(8,128)(2,1)} %up_ref.1, bf16[4,128,2048]{2,1,0:T(8,128)(2,1)} %down_ref.1, ...), custom_call_target="tpu_custom_call" | custom-call | tf_op jit(solution)/shard_map/pallas_call | solution.py:168
  170.3 4.5 %dynamic-slice_bitcast_fusion = bf16[8,2,256,512]{3,2,1,0:T(8,128)(2,1)} fusion(bf16[8,2,2,256,512]{4,3,2,1,0:T(8,128)(2,1)} %bitcast.156, s32[]{:T(128)S(6)} %select_n.239), kind=kLoop, calls=%fused_computation.2 | loop fusion | bytes 8388612 | tf_op jit(solution)/shard_map/jit(dynamic_index_in_dim)/squeeze | solution.py:112
  174.9 0.2 collective-permute-start
  175.1 0.6 dynamic_slice.124
  186.3 0.8 fusion.62
  189.0 4.8 %fusion = bf16[8,2,256,512]{3,2,1,0:T(8,128)(2,1)S(1)} fusion(bf16[8,2,256,512]{3,2,1,0:T(8,128)(2,1)} %collective-permute-done, bf16[8,2,2,256,512]{4,3,2,1,0:T(8,128)(2,1)} %bitcast.157, s32[]{:T(128)S(6)} %select_n.238), kind=kLoop, calls=%fused_computation.1 | loop fusion | flops 8388608 | bytes 12582916 | tf_op jit(solution)/shard_map/convert_element_type | solution.py:103
  193.8 1.6 fusion.59
  195.5 1.3 copy-done.1
  196.8 1.6 collective-permute-start.1
  200.3 1.7 dynamic-slice_bitcast_fusion.1
  202.0 0.5 collective-permute-start.8
  206.4 1.1 fusion.25
  207.5 1.6 collective-permute-start.2
  209.1 1.4 collective-permute-done.8
  210.5 1.8 fusion.18
  212.3 0.5 collective-permute-start.9
  216.4 1.1 fusion.24
  217.5 1.6 collective-permute-start.3
  219.1 0.8 collective-permute-done.9
  219.9 1.8 fusion.17
  221.7 0.5 collective-permute-start.10
  226.2 1.1 fusion.23
  227.3 1.6 collective-permute-start.4
  228.9 1.8 fusion.16
  230.7 0.5 collective-permute-start.11
  234.8 1.1 fusion.22
  235.9 1.6 collective-permute-start.5
  237.5 1.8 fusion.15
  239.3 0.5 collective-permute-start.12
  243.8 1.1 fusion.21
  244.9 1.6 collective-permute-start.6
  246.5 1.8 fusion.14
  248.3 0.5 collective-permute-start.13
  252.5 1.1 fusion.20
  253.6 1.6 collective-permute-start.7
  255.2 1.8 fusion.13
  257.0 0.5 collective-permute-start.14
  261.0 1.1 fusion.19
  262.1 1.6 collective-permute-done.14
  263.7 1.1 fusion.12
  264.8 0.7 copy-done.3
  265.5 0.7 fusion.30
  266.2 1.4 collective-permute-start.15
  267.6 5.3 %collective-permute-done.15 = bf16[256,512]{1,0:T(8,128)(2,1)} collective-permute-done((bf16[256,512]{1,0:T(8,128)(2,1)}, bf16[256,512]{1,0:T(8,128)(2,1)}, u32[]{:S(2)}, u32[]{:S(2)}) %collective-permute-start.15) | collective-permute-done | bytes 262176 | tf_op jit(solution)/shard_map/ppermute | solution.py:137
  272.9 1.9 fusion.11
  (63 shorter events, 1.9 us)
Async XLA Ops:
  6.5 54.3 %copy-start = (bf16[768,2048]{1,0:T(8,128)(2,1)S(1)}, bf16[768,2048]{1,0:T(8,128)(2,1)}, u32[]{:S(2)}) copy-start(bf16[768,2048]{1,0:T(8,128)(2,1)} %param.31) | copy-start | bytes 9437188
  6.5 44.0 %copy-start.6 = (f32[2,256]{1,0:T(2,128)S(1)}, f32[2,256]{1,0:T(2,128)}, u32[]{:S(2)}) copy-start(f32[2,256]{1,0:T(2,128)} %param.26) | copy-start | bytes 6148
  6.5 137.6 %all-gather.3.cloned.1.call-start = ((), (), s32[]{:S(2)}) async-start(), calls=%async_computation | async-start | bytes 8650752 | tf_op jit(solution)/shard_map/all_gather | solution.py:159
  12.3 41.0 %copy-start.7 = (f32[192]{0:T(256)S(1)}, f32[192]{0:T(256)}, u32[]{:S(2)}) copy-start(f32[192]{0:T(256)} %param.30) | copy-start | bytes 2308
  46.4 0.9 copy-start.2
  60.8 3.7 %copy-start.5 = (f32[2048]{0:T(1024)S(1)}, f32[2048]{0:T(1024)}, u32[]{:S(2)}) copy-start(f32[2048]{0:T(1024)} %param.33) | copy-start | bytes 24580
  170.3 4.8 %copy-start.8 = (s32[8]{0:T(128)S(1)}, s32[8]{0:T(128)}, u32[]{:S(2)}) copy-start(s32[8]{0:T(128)} %constant.258.clone) | copy-start | bytes 100
  170.3 16.0 %copy-start.4 = (s32[8]{0:T(128)S(1)}, s32[8]{0:T(128)}, u32[]{:S(2)}) copy-start(s32[8]{0:T(128)} %constant.259.clone) | copy-start | bytes 100
  174.9 14.1 %collective-permute-start = (bf16[8,2,256,512]{3,2,1,0:T(8,128)(2,1)}, bf16[8,2,256,512]{3,2,1,0:T(8,128)(2,1)}, u32[]{:S(2)}, u32[]{:S(2)}) collective-permute-start(bf16[8,2,256,512]{3,2,1,0:T(8,128)(2,1)} %dynamic-slice_bitcast_fusion), channel_id=1, source_target_pairs={{0,1},{1,0},{2,3},{3,2},{4,5},{5,4},{6,7},{7,6},{8,9},{9,8},{10,11... | collective-permute-start | bytes 12582920 | tf_op jit(solution)/shard_map/ppermute | solution.py:114
  195.5 1.3 copy-start.1
  196.8 9.6 %collective-permute-start.1 = (bf16[2,128,512]{2,1,0:T(8,128)(2,1)S(1)}, bf16[2,128,512]{2,1,0:T(8,128)(2,1)}, u32[]{:S(2)}, u32[]{:S(2)}) collective-permute-start(bf16[2,128,512]{2,1,0:T(8,128)(2,1)S(1)} %dynamic-slice_bitcast_fusion.2), channel_id=1, source_target_pairs={{0,8},{8,16},{16,24},{24,28},{28,20},{20,12},{12,4},{4,0},{1,9},{9... | collective-permute-start | bytes 786440 | tf_op jit(solution)/shard_map/ppermute | solution.py:131
  202.0 8.5 %collective-permute-start.8 = (bf16[2,128,512]{2,1,0:T(8,128)(2,1)}, bf16[2,128,512]{2,1,0:T(8,128)(2,1)}, u32[]{:S(2)}, u32[]{:S(2)}) collective-permute-start(bf16[2,128,512]{2,1,0:T(8,128)(2,1)} %dynamic-slice_bitcast_fusion.1), channel_id=1, source_target_pairs={{0,4},{8,0},{16,8},{24,16},{28,24},{20,28},{12,20},{4,12},{1,5},{9... | collective-permute-start | bytes 786440 | tf_op jit(solution)/shard_map/ppermute | solution.py:131
  207.5 8.9 %collective-permute-start.2 = (bf16[2,128,512]{2,1,0:T(8,128)(2,1)S(1)}, bf16[2,128,512]{2,1,0:T(8,128)(2,1)}, u32[]{:S(2)}, u32[]{:S(2)}) collective-permute-start(bf16[2,128,512]{2,1,0:T(8,128)(2,1)S(1)} %fusion.25), channel_id=1, source_target_pairs={{0,8},{8,16},{16,24},{24,28},{28,20},{20,12},{12,4},{4,0},{1,9},{9... | collective-permute-start | bytes 786440 | tf_op jit(solution)/shard_map/ppermute | solution.py:131
  212.3 7.6 %collective-permute-start.9 = (bf16[2,128,512]{2,1,0:T(8,128)(2,1)}, bf16[2,128,512]{2,1,0:T(8,128)(2,1)}, u32[]{:S(2)}, u32[]{:S(2)}) collective-permute-start(bf16[2,128,512]{2,1,0:T(8,128)(2,1)} %fusion.18), channel_id=1, source_target_pairs={{0,4},{8,0},{16,8},{24,16},{28,24},{20,28},{12,20},{4,12},{1,5},{9... | collective-permute-start | bytes 786440 | tf_op jit(solution)/shard_map/ppermute | solution.py:131
  217.5 8.6 %collective-permute-start.3 = (bf16[2,128,512]{2,1,0:T(8,128)(2,1)S(1)}, bf16[2,128,512]{2,1,0:T(8,128)(2,1)}, u32[]{:S(2)}, u32[]{:S(2)}) collective-permute-start(bf16[2,128,512]{2,1,0:T(8,128)(2,1)S(1)} %fusion.24), channel_id=1, source_target_pairs={{0,8},{8,16},{16,24},{24,28},{28,20},{20,12},{12,4},{4,0},{1,9},{9... | collective-permute-start | bytes 786440 | tf_op jit(solution)/shard_map/ppermute | solution.py:131
  221.7 7.1 %collective-permute-start.10 = (bf16[2,128,512]{2,1,0:T(8,128)(2,1)}, bf16[2,128,512]{2,1,0:T(8,128)(2,1)}, u32[]{:S(2)}, u32[]{:S(2)}) collective-permute-start(bf16[2,128,512]{2,1,0:T(8,128)(2,1)} %fusion.17), channel_id=1, source_target_pairs={{0,4},{8,0},{16,8},{24,16},{28,24},{20,28},{12,20},{4,12},{1,5},{9... | collective-permute-start | bytes 786440 | tf_op jit(solution)/shard_map/ppermute | solution.py:131
  227.3 7.5 %collective-permute-start.4 = (bf16[2,128,512]{2,1,0:T(8,128)(2,1)S(1)}, bf16[2,128,512]{2,1,0:T(8,128)(2,1)}, u32[]{:S(2)}, u32[]{:S(2)}) collective-permute-start(bf16[2,128,512]{2,1,0:T(8,128)(2,1)S(1)} %fusion.23), channel_id=1, source_target_pairs={{0,8},{8,16},{16,24},{24,28},{28,20},{20,12},{12,4},{4,0},{1,9},{9... | collective-permute-start | bytes 786440 | tf_op jit(solution)/shard_map/ppermute | solution.py:131
  230.7 6.8 %collective-permute-start.11 = (bf16[2,128,512]{2,1,0:T(8,128)(2,1)}, bf16[2,128,512]{2,1,0:T(8,128)(2,1)}, u32[]{:S(2)}, u32[]{:S(2)}) collective-permute-start(bf16[2,128,512]{2,1,0:T(8,128)(2,1)} %fusion.16), channel_id=1, source_target_pairs={{0,4},{8,0},{16,8},{24,16},{28,24},{20,28},{12,20},{4,12},{1,5},{9... | collective-permute-start | bytes 786440 | tf_op jit(solution)/shard_map/ppermute | solution.py:131
  235.9 7.8 %collective-permute-start.5 = (bf16[2,128,512]{2,1,0:T(8,128)(2,1)S(1)}, bf16[2,128,512]{2,1,0:T(8,128)(2,1)}, u32[]{:S(2)}, u32[]{:S(2)}) collective-permute-start(bf16[2,128,512]{2,1,0:T(8,128)(2,1)S(1)} %fusion.22), channel_id=1, source_target_pairs={{0,8},{8,16},{16,24},{24,28},{28,20},{20,12},{12,4},{4,0},{1,9},{9... | collective-permute-start | bytes 786440 | tf_op jit(solution)/shard_map/ppermute | solution.py:131
  239.3 7.2 %collective-permute-start.12 = (bf16[2,128,512]{2,1,0:T(8,128)(2,1)}, bf16[2,128,512]{2,1,0:T(8,128)(2,1)}, u32[]{:S(2)}, u32[]{:S(2)}) collective-permute-start(bf16[2,128,512]{2,1,0:T(8,128)(2,1)} %fusion.15), channel_id=1, source_target_pairs={{0,4},{8,0},{16,8},{24,16},{28,24},{20,28},{12,20},{4,12},{1,5},{9... | collective-permute-start | bytes 786440 | tf_op jit(solution)/shard_map/ppermute | solution.py:131
  244.9 7.6 %collective-permute-start.6 = (bf16[2,128,512]{2,1,0:T(8,128)(2,1)S(1)}, bf16[2,128,512]{2,1,0:T(8,128)(2,1)}, u32[]{:S(2)}, u32[]{:S(2)}) collective-permute-start(bf16[2,128,512]{2,1,0:T(8,128)(2,1)S(1)} %fusion.21), channel_id=1, source_target_pairs={{0,8},{8,16},{16,24},{24,28},{28,20},{20,12},{12,4},{4,0},{1,9},{9... | collective-permute-start | bytes 786440 | tf_op jit(solution)/shard_map/ppermute | solution.py:131
  248.3 6.9 %collective-permute-start.13 = (bf16[2,128,512]{2,1,0:T(8,128)(2,1)}, bf16[2,128,512]{2,1,0:T(8,128)(2,1)}, u32[]{:S(2)}, u32[]{:S(2)}) collective-permute-start(bf16[2,128,512]{2,1,0:T(8,128)(2,1)} %fusion.14), channel_id=1, source_target_pairs={{0,4},{8,0},{16,8},{24,16},{28,24},{20,28},{12,20},{4,12},{1,5},{9... | collective-permute-start | bytes 786440 | tf_op jit(solution)/shard_map/ppermute | solution.py:131
  253.6 7.4 %collective-permute-start.7 = (bf16[2,128,512]{2,1,0:T(8,128)(2,1)S(1)}, bf16[2,128,512]{2,1,0:T(8,128)(2,1)}, u32[]{:S(2)}, u32[]{:S(2)}) collective-permute-start(bf16[2,128,512]{2,1,0:T(8,128)(2,1)S(1)} %fusion.20), channel_id=1, source_target_pairs={{0,8},{8,16},{16,24},{24,28},{28,20},{20,12},{12,4},{4,0},{1,9},{9... | collective-permute-start | bytes 786440 | tf_op jit(solution)/shard_map/ppermute | solution.py:131
  257.0 6.7 %collective-permute-start.14 = (bf16[2,128,512]{2,1,0:T(8,128)(2,1)}, bf16[2,128,512]{2,1,0:T(8,128)(2,1)}, u32[]{:S(2)}, u32[]{:S(2)}) collective-permute-start(bf16[2,128,512]{2,1,0:T(8,128)(2,1)} %fusion.13), channel_id=1, source_target_pairs={{0,4},{8,0},{16,8},{24,16},{28,24},{20,28},{12,20},{4,12},{1,5},{9... | collective-permute-start | bytes 786440 | tf_op jit(solution)/shard_map/ppermute | solution.py:131
  264.8 0.7 copy-start.3
  266.2 6.7 %collective-permute-start.15 = (bf16[256,512]{1,0:T(8,128)(2,1)}, bf16[256,512]{1,0:T(8,128)(2,1)}, u32[]{:S(2)}, u32[]{:S(2)}) collective-permute-start(bf16[256,512]{1,0:T(8,128)(2,1)} %fusion.30), channel_id=1, source_target_pairs={{0,2},{1,3},{2,0},{3,1},{4,6},{5,7},{6,4},{7,5},{8,10},{9,11},{10,... | collective-permute-start | bytes 786440 | tf_op jit(solution)/shard_map/ppermute | solution.py:137
Sparse Core Ops, SparseCore 0:
  66.5 77.5 all-gather.2
